TPU v7x, 32 devices: a whole 2x2x4 slice. The times are simulated.
32 devices in a mesh: ep: 8 (over z, x), tp: 4 (over y, core).
Axes of the slice: x: 2, y: 2, z: 4, core: 2. Of those that a mesh axis runs over, the one named last changes fastest.
Arguments:
- stream: bfloat16 [128, 4096], P(None, 'ep'), may hold values from -6.5 to 6.5
- norm_gain: float32 [4096], P('ep'), may hold values from 0.1 to 1.9
- w_query: bfloat16 [4096, 2048], P('ep', 'tp'), may hold values from -0.09375 to 0.09375
- w_key: bfloat16 [4096, 1024], P('ep', 'tp'), may hold values from -0.09375 to 0.09375
- w_value: bfloat16 [4096, 1024], P('ep', 'tp'), may hold values from -0.09375 to 0.09375
- break_offset: float32 [16], P('tp'), may hold values from -10 to -2
- cache_keys: bfloat16 [128, 1024, 8, 128], P('ep', None, 'tp'), may hold values from -6 to 6
- cache_values: bfloat16 [128, 1024, 8, 128], P('ep', None, 'tp'), may hold values from -6 to 6
- lengths: int32 [128], P('ep'), may hold values from 128 to 1024
- w_output: bfloat16 [2048, 4096], P('tp', 'ep'), may hold values from -0.125 to 0.125
- head_gain: float32 [2048], P('tp'), may hold values from 0.1 to 1.9
- ffn_gain: float32 [4096], P('ep'), may hold values from 0.1 to 1.9
- route_experts: int32 [128, 2], replicated, may hold values from 0 to 7, all different within a row; in each aligned block of 128 rows (0 to 127, 128 to 255, ...) at most 64 rows name the same one
- route_weights: float32 [128, 2], replicated, may hold values from 0.1 to 1
- expert_gate: bfloat16 [8, 4096, 1024], P('ep', None, 'tp'), may hold values from -0.09375 to 0.09375
- expert_up: bfloat16 [8, 4096, 1024], P('ep', None, 'tp'), may hold values from -0.09375 to 0.09375
- expert_down: bfloat16 [8, 1024, 4096], P('ep', 'tp'), may hold values from -0.1875 to 0.1875
- dense_gate: bfloat16 [4096, 4096], P('ep', 'tp'), may hold values from -0.09375 to 0.09375
- dense_up: bfloat16 [4096, 4096], P('ep', 'tp'), may hold values from -0.09375 to 0.09375
- dense_down: bfloat16 [4096, 4096], P('tp', 'ep'), may hold values from -0.09375 to 0.09375
- mix_gain: float32 [4096], P('ep'), may hold values from 0.1 to 1.9
Outputs:
- mixed_out: bfloat16 [128, 4096], P(None, 'ep')
- key_rows: bfloat16 [128, 1024], P('ep', 'tp')
- value_rows: bfloat16 [128, 1024], P('ep', 'tp')
Inputs may be any that keep to these rules, and one draw needn't show every extreme that they name: `route_experts`: in the whole batch no expert is named by more than 64 pairs, a bound that some block reaches; the 2 experts of a token differ.
All inputs are finite; a program needn't handle non-finite values.
Results may differ from a plain program's by a relative error of at most 0.025.
Values may be sent and summed in bfloat16 or wider, within the bound.
A program may use at most 64 MiB of HBM per device.

v0:
```python
import functools

import jax
import jax.numpy as jnp
from jax import lax
from jax.experimental import pallas as pl
from jax.experimental.pallas import tpu as pltpu
from jax.sharding import PartitionSpec as P

EPSILON = 1e-06
MESH = pl.DeviceIdType.MESH
F32 = jnp.float32
BF16 = jnp.bfloat16
NT = (((1,), (1,)), ((), ()))


def row_sums(squares):
    ones = jnp.ones((8, squares.shape[1]), BF16)
    high = squares.astype(BF16)
    low = (squares - high.astype(F32)).astype(BF16)
    return lax.dot_general(ones, high, NT, preferred_element_type=F32) + lax.dot_general(
        ones, low, NT, preferred_element_type=F32
    )


def own_column(sums, first, rows):
    width = sums.shape[1]
    lane = lax.broadcasted_iota(jnp.int32, (rows, width), 1)
    row = lax.broadcasted_iota(jnp.int32, (rows, width), 0)
    return jnp.sum(jnp.where(lane == row + first, sums[0:1, :], 0.0), axis=1, keepdims=True)


def greet(axes):
    barrier = pltpu.get_barrier_semaphore()
    total = 0
    for axis, count in axes:
        me = lax.axis_index(axis)
        for k in range(1, count):
            pl.semaphore_signal(
                barrier, inc=1, device_id={axis: lax.rem(me + k, count)}, device_id_type=MESH
            )
            total += 1
    pl.semaphore_wait(barrier, total)


def send(axis, count, k, src, dst, send_sem, recv_sem):
    peer = lax.rem(lax.axis_index(axis) + k, count)
    copy = pltpu.make_async_remote_copy(
        src_ref=src,
        dst_ref=dst,
        send_sem=send_sem.at[k - 1],
        recv_sem=recv_sem.at[k - 1],
        device_id={axis: peer},
        device_id_type=MESH,
    )
    copy.start()
    return copy


def send_to(peer, src, dst, sems, i):
    copy = pltpu.make_async_remote_copy(
        src_ref=src,
        dst_ref=dst,
        send_sem=sems[0].at[i],
        recv_sem=sems[1].at[i],
        device_id={"tp": peer},
        device_id_type=MESH,
    )
    copy.start()
    return copy


def tp_sum(nt, part, arrived, pair, crossed, full, sems, extra):
    me = lax.axis_index("tp")
    core = lax.rem(me, 2)
    partner = me + 1 - 2 * core
    half = pair.shape[0]
    mine = pl.ds(pl.multiple_of(core * half, half), half)
    other = pl.ds(pl.multiple_of((1 - core) * half, half), half)
    copies = [send_to(partner, part.at[other], arrived, sems, 0)]
    copies[0].wait_recv()
    pair[...] = (part[mine].astype(F32) + arrived[...].astype(F32)).astype(BF16)
    for j in range(1, nt // 2):
        copies.append(send_to(lax.rem(me + 2 * j, nt), pair, crossed.at[j - 1], sems, j))
    total = pair[...].astype(F32)
    for j in range(1, nt // 2):
        copies[j].wait_recv()
        total = total + crossed[j - 1].astype(F32)
    if extra is not None:
        total = total + extra[mine]
    full[mine] = total.astype(BF16)
    copies.append(send_to(partner, full.at[mine], full.at[mine], sems, nt // 2))
    copies[-1].wait_recv()
    for copy in copies:
        copy.wait_send()


def project_kernel(
    n, width, x_ref, g_ref, wq_ref, wk_ref, wv_ref, q_ref, k_ref, v_ref,
    part, sums, got, got_sums, s_send, s_recv, p_send, p_recv,
):
    me = lax.axis_index("ep")
    x = x_ref[...].astype(F32)
    xg = (x * g_ref[...]).astype(BF16)
    rows = k_ref.shape[0]
    sums[...] = row_sums(x * x)
    at = 0
    for w_ref in (wq_ref, wk_ref, wv_ref):
        cols = w_ref.shape[1]
        val = jnp.dot(xg, w_ref[...], preferred_element_type=F32).astype(BF16)
        for i in range(n):
            part[i, :, at : at + cols] = val[i * rows : (i + 1) * rows]
        at += cols
    greet((("ep", n),))
    copies = []
    for k in range(1, n):
        peer = lax.rem(me + k, n)
        copies.append(send("ep", n, k, part.at[peer], got.at[k - 1], p_send, p_recv))
        copies.append(send("ep", n, k, sums, got_sums.at[k - 1], s_send, s_recv))
    total = part[me].astype(F32)
    squares = sums[...]
    for k in range(1, n):
        copies[2 * k - 2].wait_recv()
        total = total + got[k - 1].astype(F32)
        copies[2 * k - 1].wait_recv()
        squares = squares + got_sums[k - 1]
    mean = own_column(squares, me * rows, rows) / width
    total = total * lax.rsqrt(mean + EPSILON)
    hd = q_ref.shape[2]
    q_width = wq_ref.shape[1]
    k_width = wk_ref.shape[1]
    for h in range(q_ref.shape[0]):
        q_ref[h] = total[:, h * hd : (h + 1) * hd].astype(BF16).astype(F32)
    k_ref[...] = total[:, q_width : q_width + k_width].astype(BF16)
    v_ref[...] = total[:, q_width + k_width :].astype(BF16)
    for copy in copies:
        copy.wait_send()


def attend_kernel(kv, per, len_ref, off_ref, q_ref, gain_ref, new_k_ref, new_v_ref, key_ref, val_ref,
                  out_ref, k_out_ref, v_out_ref):
    step = pl.program_id(0)
    k_out_ref[...] = new_k_ref[...]
    v_out_ref[...] = new_v_ref[...]
    heads = q_ref.shape[0]
    hd = q_ref.shape[2]
    cols = key_ref.shape[1]
    group = heads // kv
    rows = per * heads
    lanes = 128
    blocks = cols // lanes
    q = jnp.concatenate(
        [q_ref[h, pl.ds(step * per + s, 1), :] for s in range(per) for h in range(heads)], axis=0
    ).astype(BF16)
    row = lax.broadcasted_iota(jnp.int32, (rows, lanes), 0)
    lane = lax.broadcasted_iota(jnp.int32, (rows, lanes), 1)
    offset = jnp.zeros((rows, lanes), F32)
    length = jnp.zeros((rows, lanes), jnp.int32)
    for s in range(per):
        length = jnp.where(row // heads == s, len_ref[step * per + s], length)
    for h in range(heads):
        offset = jnp.where(row % heads == h, off_ref[h], offset)
    mine = (row % heads) // group
    scores = jnp.zeros((rows, cols), F32)
    row_all = lax.broadcasted_iota(jnp.int32, (rows, cols), 0)
    for s in range(per):
        one = lax.dot_general(q, key_ref[s], NT, preferred_element_type=F32)
        scores = one if s == 0 else jnp.where(row_all // heads == s, one, scores)
    sigs, valids, fails = [], [], []
    for b in range(blocks):
        sc = scores[:, b * lanes : (b + 1) * lanes] * hd ** (-0.5) + offset
        col = lane + b * lanes
        valid = (col // kv < length) & (col % kv == mine)
        ls = jnp.minimum(sc, 0.0) - jnp.log(1.0 + jnp.exp(-jnp.abs(sc)))
        sigs.append(ls)
        valids.append(valid)
        fails.append(jnp.where(valid, ls - sc, 0.0))
    failed = jnp.concatenate(fails, axis=0)
    high = failed.astype(BF16)
    low = (failed - high.astype(F32)).astype(BF16)
    r = lax.broadcasted_iota(jnp.int32, (lanes, 2 * lanes), 0)
    c = lax.broadcasted_iota(jnp.int32, (lanes, 2 * lanes), 1)
    tri = jnp.where((r > c) | (c >= lanes), 1.0, 0.0).astype(BF16)
    sums = jnp.dot(high, tri, preferred_element_type=F32) + jnp.dot(
        low, tri, preferred_element_type=F32
    )
    acc = jnp.zeros((rows, lanes), F32)
    weights = [None] * blocks
    for b in reversed(range(blocks)):
        later = sums[b * rows : (b + 1) * rows, :lanes] + acc
        acc = acc + sums[b * rows : (b + 1) * rows, lanes:]
        weights[b] = jnp.where(valids[b], jnp.exp(sigs[b] + later), 0.0)
    weights = jnp.concatenate(weights, axis=1).astype(BF16)
    row_out = lax.broadcasted_iota(jnp.int32, (rows, hd), 0)
    att = None
    for s in range(per):
        one = jnp.dot(weights, val_ref[s], preferred_element_type=F32)
        att = one if s == 0 else jnp.where(row_out // heads == s, one, att)
    gains = jnp.concatenate([gain_ref[...]] * per, axis=0)
    att = att * lax.rsqrt(jnp.mean(att * att, axis=1, keepdims=True) + EPSILON) * gains
    for s in range(per):
        for h in range(heads):
            out_ref[h, pl.ds(step * per + s, 1), :] = att[s * heads + h : s * heads + h + 1]


def rest_kernel(
    n, nt, width, cap,
    head_ref, x_ref, fg_ref, mix_ref, route_ref, route_w_ref,
    wo_hbm, dg_hbm, du_hbm, dd_hbm, eg_hbm, eu_hbm, ed_hbm,
    out_ref,
    wo, dg, du, dd, eg, eu, ed, w_sem,
    heads_all, part, disp, disp_in, sums, sums_in, gu, gu_in, hid_all, act_s, share_s,
    ret_x, ret_p, ret_m, ret, ret_in, res,
    a_in, a_pair, a_cross, a_full, f_in, f_pair, f_cross, f_full,
    h_send, h_recv, d_send, d_recv, w_send, w_recv, s_send, s_recv, g_send, g_recv,
    i_send, i_recv, r_send, r_recv, a_send, a_recv, f_send, f_recv, x_send, x_recv,
):
    me = lax.axis_index("ep")
    loads = []
    for i, (src, dst) in enumerate(
        ((wo_hbm, wo), (dg_hbm, dg), (du_hbm, du), (eg_hbm.at[0], eg), (eu_hbm.at[0], eu),
         (ed_hbm.at[0], ed), (dd_hbm, dd))
    ):
        load = pltpu.make_async_copy(src, dst, w_sem.at[i])
        load.start()
        loads.append(load)
    total_rows, block = x_ref.shape
    rows = total_rows // n
    heads_all[me] = jnp.concatenate(
        [head_ref[h] for h in range(head_ref.shape[0])], axis=1
    ).astype(BF16)
    greet((("ep", n), ("tp", nt)))
    sent = []
    copies = [
        send("ep", n, k, heads_all.at[me], heads_all.at[me], h_send, h_recv) for k in range(1, n)
    ]
    sent += copies
    me_t = lax.axis_index("tp")
    core = lax.rem(me_t, 2)
    partner = me_t + 1 - 2 * core
    half = cap // 2
    near = pl.ds(pl.multiple_of(core * half, half), half)
    far = pl.ds(pl.multiple_of((1 - core) * half, half), half)
    top = route_ref.shape[0]
    expert_ids = lax.broadcasted_iota(jnp.int32, (n, total_rows), 0)
    named = [
        jnp.where(route_ref[k : k + 1, :] == expert_ids, 1.0, 0.0).astype(F32)
        for k in range(top)
    ]
    token_r = lax.broadcasted_iota(jnp.int32, (total_rows, total_rows), 0)
    token_c = lax.broadcasted_iota(jnp.int32, (total_rows, total_rows), 1)
    before = jnp.dot(
        sum(named).astype(BF16),
        jnp.where(token_r < token_c, 1.0, 0.0).astype(BF16),
        preferred_element_type=F32,
    )
    slots = [
        jnp.sum(named[k] * before, axis=0, keepdims=True)
        + route_ref[k : k + 1, :].astype(F32) * cap
        for k in range(top)
    ]
    columns = [
        jnp.sum(jnp.where(token_r == token_c, slot, 0.0), axis=1, keepdims=True)
        for slot in slots
    ]
    share_sum = route_w_ref[0:1, :]
    for k in range(1, top):
        share_sum = share_sum + route_w_ref[k : k + 1, :]
    share_rows = [route_w_ref[k : k + 1, :] / share_sum for k in range(top)]
    slot_rows = lax.broadcasted_iota(jnp.int32, (cap, total_rows), 0)
    half_rows = lax.broadcasted_iota(jnp.int32, (half, total_rows), 0) + core * half
    loads[0].wait()
    for copy in copies:
        copy.wait_recv()
    all_heads = heads_all[...].reshape(total_rows, heads_all.shape[2])
    part[...] = jnp.dot(all_heads, wo[...], preferred_element_type=F32).astype(BF16)
    tp_sum(nt, part, a_in, a_pair, a_cross, a_full, (a_send, a_recv), None)
    residual = x_ref[...].astype(F32) + a_full[...].astype(F32)
    u = (residual * fg_ref[...]).astype(BF16)
    sums[...] = row_sums(residual * residual)
    res[...] = residual

    def picks(expert, places):
        place = (places + expert * cap).astype(F32)
        return [slot == place for slot in slots]

    d_copies, s_copies = [], []
    for k in range(1, n):
        peer = lax.rem(me + k, n)
        hit = functools.reduce(jnp.logical_or, picks(peer, half_rows))
        disp[k] = jnp.dot(
            jnp.where(hit, 1.0, 0.0).astype(BF16), u, preferred_element_type=F32
        ).astype(BF16)
        d_copies.append(send("ep", n, k, disp.at[k], disp_in.at[k - 1, near], d_send, d_recv))
        s_copies.append(send("ep", n, k, sums, sums_in.at[k - 1], s_send, s_recv))
    sent += d_copies + s_copies
    mine = picks(me, slot_rows)
    hit = functools.reduce(jnp.logical_or, mine)
    own_in = jnp.dot(
        jnp.where(hit, 1.0, 0.0).astype(BF16), u, preferred_element_type=F32
    ).astype(BF16)
    hidden = dg.shape[1]
    loads[1].wait()
    val = jnp.dot(u, dg[...], preferred_element_type=F32).astype(BF16)
    for i in range(n):
        gu[i, :, :hidden] = val[i * rows : (i + 1) * rows]
    loads[2].wait()
    val = jnp.dot(u, du[...], preferred_element_type=F32).astype(BF16)
    for i in range(n):
        gu[i, :, hidden:] = val[i * rows : (i + 1) * rows]
    g_copies = [
        send("ep", n, k, gu.at[lax.rem(me + k, n)], gu_in.at[k - 1], g_send, g_recv)
        for k in range(1, n)
    ]
    sent += g_copies
    loads[3].wait()
    loads[4].wait()
    first = pl.ds(pl.multiple_of(me * block, block), block)
    gate = jnp.dot(own_in, eg[first, :], preferred_element_type=F32)
    up = jnp.dot(own_in, eu[first, :], preferred_element_type=F32)
    squares = sums[...]
    forwards = []
    for k in range(1, n + 1):
        if k < n:
            d_copies[k - 1].wait_recv()
            forwards.append(
                send_to(
                    partner, disp_in.at[k - 1, near], disp_in.at[k - 1, near],
                    (w_send, w_recv), k - 1,
                )
            )
        if k > 1:
            p = k - 1
            s_copies[p - 1].wait_recv()
            squares = squares + sums_in[p - 1]
            forwards[p - 1].wait_recv()
            owner = lax.rem(me - p + n, n)
            span = pl.ds(pl.multiple_of(owner * block, block), block)
            gate = gate + jnp.dot(disp_in[p - 1], eg[span, :], preferred_element_type=F32)
            up = up + jnp.dot(disp_in[p - 1], eu[span, :], preferred_element_type=F32)
    sent += forwards
    scale_row = lax.rsqrt(squares[0:1, :] / width + EPSILON)
    scale = jnp.sum(jnp.where(hit, scale_row, 0.0), axis=1, keepdims=True)
    share = jnp.zeros((cap, 1), F32)
    for k in range(len(mine)):
        share = share + jnp.sum(
            jnp.where(mine[k], share_rows[k], 0.0), axis=1, keepdims=True
        )
    gate = gate * scale
    up = up * scale
    act_s[...] = (gate / (1.0 + jnp.exp(-gate)) * up).astype(BF16)
    share_s[...] = jnp.broadcast_to(share, share_s.shape)
    loads[5].wait()
    act_far = act_s[far]
    share_far = share_s[far][:, 0:1]
    for i in range(n):
        ret_x[i] = (
            jnp.dot(act_far, ed[:, i * block : (i + 1) * block], preferred_element_type=F32)
            * share_far
        ).astype(BF16)
    swap = send_to(partner, ret_x, ret_p, (x_send, x_recv), 0)
    sent.append(swap)
    act_near = act_s[near]
    share_near = share_s[near][:, 0:1]
    for i in range(n):
        ret_m[i] = (
            jnp.dot(act_near, ed[:, i * block : (i + 1) * block], preferred_element_type=F32)
            * share_near
        )
    swap.wait_recv()
    for i in range(n):
        ret[i] = (ret_m[i] + ret_p[i].astype(F32)).astype(BF16)
    r_copies = [
        send("ep", n, k, ret.at[lax.rem(me + k, n)], ret_in.at[k - 1], r_send, r_recv)
        for k in range(1, n)
    ]
    sent += r_copies
    gate_up = gu[me].astype(F32)
    for k in range(1, n):
        g_copies[k - 1].wait_recv()
        gate_up = gate_up + gu_in[k - 1].astype(F32)
    gate_up = gate_up * own_column(
        jnp.broadcast_to(scale_row, (8, total_rows)), me * rows, rows
    )
    dense_gate = gate_up[:, :hidden]
    hid_all[me] = (dense_gate / (1.0 + jnp.exp(-dense_gate)) * gate_up[:, hidden:]).astype(BF16)
    i_copies = [
        send("ep", n, k, hid_all.at[me], hid_all.at[me], i_send, i_recv) for k in range(1, n)
    ]
    sent += i_copies
    slot_cols = lax.broadcasted_iota(jnp.int32, (total_rows, half), 1) + core * half
    def combine(expert, rows_in):
        place = (slot_cols + expert * cap).astype(F32)
        hits = functools.reduce(jnp.logical_or, [column == place for column in columns])
        return jnp.dot(
            jnp.where(hits, 1.0, 0.0).astype(BF16), rows_in, preferred_element_type=F32
        )

    moe = combine(me, ret[me])
    for k in range(1, n):
        r_copies[k - 1].wait_recv()
        moe = moe + combine(lax.rem(me - k + n, n), ret_in[k - 1])
    loads[6].wait()
    for copy in i_copies:
        copy.wait_recv()
    dense = jnp.dot(
        hid_all[...].reshape(total_rows, hidden), dd[...], preferred_element_type=F32
    )
    both = moe + mix_ref[...] * dense
    part[...] = both.astype(BF16)
    tp_sum(nt, part, f_in, f_pair, f_cross, f_full, (f_send, f_recv), res)
    out_ref[...] = f_full[...]
    for copy in sent:
        copy.wait_send()


def per_device(
    n, nt, stream, norm_gain, w_query, w_key, w_value, break_offset, cache_keys, cache_values,
    lengths, w_output, head_gain, ffn_gain, route_experts, route_weights, expert_gate,
    expert_up, expert_down, dense_gate, dense_up, dense_down, mix_gain,
):
    total_rows, block = stream.shape
    width = block * n
    rows = lengths.shape[0]
    kv = cache_keys.shape[2]
    hd = cache_keys.shape[3]
    heads = break_offset.shape[0]
    cache_len = cache_keys.shape[1]
    top = route_experts.shape[1]
    hidden = dense_gate.shape[1]
    expert_hidden = expert_gate.shape[2]
    experts = expert_gate.shape[0] * n
    cap = 2 * rows * top // expert_gate.shape[0]
    assert experts == n
    vmem = pl.BlockSpec(memory_space=pltpu.VMEM)
    hbm = pl.BlockSpec(memory_space=pl.ANY)
    dma = pltpu.SemaphoreType.DMA
    limit = 60 * 1024 * 1024

    wide = w_query.shape[1] + w_key.shape[1] + w_value.shape[1]
    queries, key_rows, value_rows = pl.pallas_call(
        functools.partial(project_kernel, n, width),
        out_shape=(
            jax.ShapeDtypeStruct((heads, rows, hd), F32),
            jax.ShapeDtypeStruct((rows, w_key.shape[1]), BF16),
            jax.ShapeDtypeStruct((rows, w_value.shape[1]), BF16),
        ),
        in_specs=[vmem] * 5,
        out_specs=(vmem, vmem, vmem),
        scratch_shapes=[
            pltpu.VMEM((n, rows, wide), BF16),
            pltpu.VMEM((8, total_rows), F32),
            pltpu.VMEM((n - 1, rows, wide), BF16),
            pltpu.VMEM((n - 1, 8, total_rows), F32),
            dma((n - 1,)), dma((n - 1,)), dma((n - 1,)), dma((n - 1,)),
        ],
        compiler_params=pltpu.CompilerParams(collective_id=0, has_side_effects=True),
        name="project",
    )(stream, norm_gain.reshape(1, block), w_query, w_key, w_value)

    per = 2
    flat = kv * cache_len
    smem = pl.BlockSpec(memory_space=pltpu.SMEM)
    k_block = pl.BlockSpec(key_rows.shape, lambda i: (0, 0))
    v_block = pl.BlockSpec(value_rows.shape, lambda i: (0, 0))
    head_out, key_rows, value_rows = pl.pallas_call(
        functools.partial(attend_kernel, kv, per),
        grid=(rows // per,),
        out_shape=(
            jax.ShapeDtypeStruct((heads, rows, hd), F32),
            jax.ShapeDtypeStruct(key_rows.shape, BF16),
            jax.ShapeDtypeStruct(value_rows.shape, BF16),
        ),
        in_specs=[
            smem,
            smem,
            pl.BlockSpec((heads, rows, hd), lambda i: (0, 0, 0)),
            pl.BlockSpec((heads, hd), lambda i: (0, 0)),
            k_block,
            v_block,
            pl.BlockSpec((per, flat, hd), lambda i: (i, 0, 0)),
            pl.BlockSpec((per, flat, hd), lambda i: (i, 0, 0)),
        ],
        out_specs=(pl.BlockSpec((heads, rows, hd), lambda i: (0, 0, 0)), k_block, v_block),
        compiler_params=pltpu.CompilerParams(dimension_semantics=("arbitrary",)),
        name="attend",
    )(
        lengths,
        break_offset,
        queries,
        head_gain.reshape(heads, hd),
        key_rows,
        value_rows,
        cache_keys.reshape(rows, flat, hd),
        cache_values.reshape(rows, flat, hd),
    )

    dt = w_output.shape[0]
    assert nt % 2 == 0 and cap % 2 == 0
    half_cap = (n, cap // 2, block)
    half_rows = (total_rows // 2, block)
    mixed_out = pl.pallas_call(
        functools.partial(rest_kernel, n, nt, width, cap),
        out_shape=jax.ShapeDtypeStruct((total_rows, block), BF16),
        in_specs=[vmem] * 6 + [hbm] * 7,
        out_specs=vmem,
        scratch_shapes=[
            pltpu.VMEM(w_output.shape, BF16),
            pltpu.VMEM(dense_gate.shape, BF16),
            pltpu.VMEM(dense_up.shape, BF16),
            pltpu.VMEM(dense_down.shape, BF16),
            pltpu.VMEM(expert_gate.shape[1:], BF16),
            pltpu.VMEM(expert_up.shape[1:], BF16),
            pltpu.VMEM(expert_down.shape[1:], BF16),
            dma((7,)),
            pltpu.VMEM((n, rows, dt), BF16),
            pltpu.VMEM((total_rows, block), BF16),
            pltpu.VMEM(half_cap, BF16),
            pltpu.VMEM((n - 1, cap, block), BF16),
            pltpu.VMEM((8, total_rows), F32),
            pltpu.VMEM((n - 1, 8, total_rows), F32),
            pltpu.VMEM((n, rows, 2 * hidden), BF16),
            pltpu.VMEM((n - 1, rows, 2 * hidden), BF16),
            pltpu.VMEM((n, rows, hidden), BF16),
            pltpu.VMEM((cap, expert_hidden), BF16),
            pltpu.VMEM((cap, 128), F32),
            pltpu.VMEM(half_cap, BF16),
            pltpu.VMEM(half_cap, BF16),
            pltpu.VMEM(half_cap, F32),
            pltpu.VMEM(half_cap, BF16),
            pltpu.VMEM((n - 1, cap // 2, block), BF16),
            pltpu.VMEM((total_rows, block), F32),
        ]
        + [
            pltpu.VMEM(half_rows, BF16),
            pltpu.VMEM(half_rows, BF16),
            pltpu.VMEM((nt // 2 - 1,) + half_rows, BF16),
            pltpu.VMEM((total_rows, block), BF16),
        ] * 2
        + [dma((n - 1,))] * 14
        + [dma((nt // 2 + 1,))] * 4
        + [
            dma((1,)),
            dma((1,)),
        ],
        compiler_params=pltpu.CompilerParams(
            collective_id=1, has_side_effects=True, vmem_limit_bytes=limit
        ),
        name="rest",
    )(
        head_out, stream, ffn_gain.reshape(1, block), mix_gain.reshape(1, block),
        route_experts.T, route_weights.T,
        w_output, dense_gate, dense_up, dense_down, expert_gate, expert_up, expert_down,
    )
    return (mixed_out, key_rows, value_rows)


def solution(mesh):
    in_specs = (
        P(None, "ep"),
        P("ep"),
        P("ep", "tp"),
        P("ep", "tp"),
        P("ep", "tp"),
        P("tp"),
        P("ep", None, "tp", None),
        P("ep", None, "tp", None),
        P("ep"),
        P("tp", "ep"),
        P("tp"),
        P("ep"),
        P(),
        P(),
        P("ep", None, "tp"),
        P("ep", None, "tp"),
        P("ep", "tp", None),
        P("ep", "tp"),
        P("ep", "tp"),
        P("tp", "ep"),
        P("ep"),
    )
    out_specs = (P(None, "ep"), P("ep", "tp"), P("ep", "tp"))
    body = functools.partial(per_device, mesh.shape["ep"], mesh.shape["tp"])
    return jax.shard_map(
        body, mesh=mesh, in_specs=in_specs, out_specs=out_specs, check_vma=False
    )
```

profile of v0, /device:TPU:0, one launch (start us, length us, event | category | flops | bytes accessed | tf_op | source)
XLA Modules:
  0.0 81.1 jit_solution(8992459079575657541)
XLA Ops:
  0.6 13.7 %project.1 = (f32[4,16,128]{2,1,0:T(8,128)}, bf16[16,256]{1,0:T(8,128)(2,1)}, bf16[16,256]{1,0:T(8,128)(2,1)}) custom-call(bf16[128,512]{1,0:T(8,128)(2,1)} %x_ref.3, f32[1,512]{1,0:T(1,128)} %bitcast.10, bf16[512,512]{1,0:T(8,128)(2,1)} %wq_ref.1, bf16[512,256]{1,0:T(8,128)(2,1)} %wk_ref.1, bf16[512,256]{1,0:T(8,128)(2,1)} %wv_ref.1), custom_call_target="tpu_custom_call" | custom-call | tf_op jit(solution)/shard_map/project/pallas_call | solution.py:441
  14.4 11.9 %attend.1 = (f32[4,16,128]{2,1,0:T(8,128)}, bf16[16,256]{1,0:T(8,128)(2,1)}, bf16[16,256]{1,0:T(8,128)(2,1)}) custom-call(s32[16]{0:T(128)} %len_ref.1, f32[4]{0:T(128)} %off_ref.1, f32[4,16,128]{2,1,0:T(8,128)} %get-tuple-element.9.q_ref, f32[4,128]{1,0:T(4,128)} %bitcast.13, bf16[16,256]{1,0:T(8,128)(2,1)} %get-tuple-element.10.new_k_ref, ...), custom_call_target="tpu_custom_call" | custom-call | tf_op jit(solution)/shard_map/attend/pallas_call | solution.py:466
  26.3 53.2 %rest.1 = bf16[128,512]{1,0:T(8,128)(2,1)} custom-call(f32[4,16,128]{2,1,0:T(8,128)} %get-tuple-element.12.head_ref, bf16[128,512]{1,0:T(8,128)(2,1)} %x_ref.3, f32[1,512]{1,0:T(1,128)} %bitcast.11, f32[1,512]{1,0:T(1,128)} %bitcast.12, s32[2,128]{1,0:T(2,128)} %bitcast.14, f32[2,128]{1,0:T(2,128)} %bitcast.15, bf16[512,512]{1,0:T(8,128)(2,1)} %wo_hbm.1, ...), custom_call_target="tpu_custom_call" | custom-call | tf_op jit(solution)/shard_map/rest/pallas_call | solution.py:502
  79.5 1.6 %copy.25 = bf16[128,512]{1,0:T(8,128)(2,1)} copy(bf16[128,512]{1,0:T(8,128)(2,1)} %rest.1) | data formatting | bytes 262144
where the time goes:
time: 81.4 us; the launch traced here: 81.1 us
  Pallas kernels  78.9 us (97%)
  local copies, waits for them, and re-layouts  1.57 us (2%)
    pallas_call x1, Pallas kernels, per_device(): pl.pallas_call(functools.partial(rest_kernel, n, nt, width, cap), out_sha...  53.2 us
    pallas_call x1, Pallas kernels, per_device(): pl.pallas_call(functools.partial(project_kernel, n, width), out_shape=(ja...  13.7 us
    pallas_call x1, Pallas kernels, per_device(): pl.pallas_call(functools.partial(attend_kernel, kv, per), grid=(rows // p...  11.9 us

commit v1 on v0

v1 whole, which is shorter than its diff:
```python
import functools

import jax
import jax.numpy as jnp
from jax import lax
from jax.experimental import pallas as pl
from jax.experimental.pallas import tpu as pltpu
from jax.sharding import PartitionSpec as P

EPSILON = 1e-06
MESH = pl.DeviceIdType.MESH
F32 = jnp.float32
BF16 = jnp.bfloat16
LIMIT_MIB = 48
NT = (((1,), (1,)), ((), ()))


def row_sums(squares):
    ones = jnp.ones((8, squares.shape[1]), BF16)
    high = squares.astype(BF16)
    low = (squares - high.astype(F32)).astype(BF16)
    return lax.dot_general(ones, high, NT, preferred_element_type=F32) + lax.dot_general(
        ones, low, NT, preferred_element_type=F32
    )


def own_column(sums, first, rows):
    width = sums.shape[1]
    lane = lax.broadcasted_iota(jnp.int32, (rows, width), 1)
    row = lax.broadcasted_iota(jnp.int32, (rows, width), 0)
    return jnp.sum(jnp.where(lane == row + first, sums[0:1, :], 0.0), axis=1, keepdims=True)


def plan(n):
    inner = 1 << ((n.bit_length() - 1) // 2)
    return n // inner, inner


def spread(count):
    return sorted(range(1, count), key=lambda d: abs(2 * d - count))


class Grid:
    def __init__(self, n):
        self.nz, self.nx = plan(n)
        self.me = lax.axis_index("ep")
        self.z = self.me // self.nx
        self.x = lax.rem(self.me, self.nx)

    def at(self, dz, dx):
        return lax.rem(self.z + dz, self.nz) * self.nx + lax.rem(self.x + dx, self.nx)

    def source(self, dz, dx):
        return self.at(self.nz - dz, self.nx - dx)

    def peers(self):
        order = spread(self.nz)
        return [(dz, dx) for dz in order for dx in range(self.nx)] + [
            (0, dx) for dx in range(1, self.nx)
        ]


def signal_all(axes):
    barrier = pltpu.get_barrier_semaphore()
    total = 0
    for axis, count in axes:
        me = lax.axis_index(axis)
        for k in range(1, count):
            pl.semaphore_signal(
                barrier, inc=1, device_id={axis: lax.rem(me + k, count)}, device_id_type=MESH
            )
            total += 1
    return barrier, total


def push(axis, peer, src, dst, sems, i):
    copy = pltpu.make_async_remote_copy(
        src_ref=src,
        dst_ref=dst,
        send_sem=sems[0].at[i],
        recv_sem=sems[1].at[i],
        device_id={axis: peer},
        device_id_type=MESH,
    )
    copy.start()
    return copy


def scatter_first(g, part, got, sems):
    copies = {}
    for dz in spread(g.nz) + [0]:
        for dx in range(1, g.nx):
            i = dz * (g.nx - 1) + dx - 1
            copies[dz, dx] = push("ep", g.at(0, dx), part.at[g.at(dz, dx)], got.at[i], sems, i)
    return copies


def scatter_next(g, part, got, copies, mid, got2, sems, dz):
    acc = part[g.at(dz, 0)].astype(F32)
    for dx in range(1, g.nx):
        copies[dz, dx].wait_recv()
        acc = acc + got[dz * (g.nx - 1) + dx - 1].astype(F32)
    if dz == 0:
        return acc
    mid[dz - 1] = acc.astype(BF16)
    return push("ep", g.at(dz, 0), mid.at[dz - 1], got2.at[dz - 1], sems, dz - 1)


def tp_sum(nt, part, arrived, pair, crossed, full, sems, extra):
    me = lax.axis_index("tp")
    core = lax.rem(me, 2)
    partner = me + 1 - 2 * core
    half = pair.shape[0]
    mine = pl.ds(pl.multiple_of(core * half, half), half)
    other = pl.ds(pl.multiple_of((1 - core) * half, half), half)
    copies = [push("tp", partner, part.at[other], arrived, sems, 0)]
    copies[0].wait_recv()
    pair[...] = (part[mine].astype(F32) + arrived[...].astype(F32)).astype(BF16)
    for j in range(1, nt // 2):
        copies.append(push("tp", lax.rem(me + 2 * j, nt), pair, crossed.at[j - 1], sems, j))
    total = pair[...].astype(F32)
    for j in range(1, nt // 2):
        copies[j].wait_recv()
        total = total + crossed[j - 1].astype(F32)
    if extra is not None:
        total = total + extra[mine]
    full[mine] = total.astype(BF16)
    copies.append(push("tp", partner, full.at[mine], full.at[mine], sems, nt // 2))
    copies[-1].wait_recv()
    return copies


def attend(kv, per, waits, len_ref, off_ref, gain_ref, q_s, k_s, v_s, sc_s, sg_s, hl_s, sm_s,
           ho_s):
    heads, rows, hd = q_s.shape
    cols = k_s.shape[1]
    group = heads // kv
    m = per * heads
    lanes = 128
    blocks = cols // lanes
    pairs = rows // per
    row_q = lax.broadcasted_iota(jnp.int32, (m, hd), 0)
    row = lax.broadcasted_iota(jnp.int32, (m, lanes), 0)
    lane = lax.broadcasted_iota(jnp.int32, (m, lanes), 1)
    for p in range(pairs):
        q = jnp.concatenate(
            [q_s[h, pl.ds(p * per + s, 1), :] for s in range(per) for h in range(heads)], axis=0
        )
        wide = jnp.concatenate(
            [jnp.where(row_q // heads == s, q, 0.0) for s in range(per)], axis=1
        ).astype(BF16)
        waits[0][p].wait()
        keys = jnp.concatenate([k_s[p * per + s] for s in range(per)], axis=1)
        sc_s[p] = lax.dot_general(wide, keys, NT, preferred_element_type=F32)
    offset = jnp.zeros((m, lanes), F32)
    for h in range(heads):
        offset = jnp.where(row % heads == h, off_ref[h], offset)
    mine = (row % heads) // group == lane % kv
    limits = []
    for p in range(pairs):
        length = jnp.zeros((m, lanes), jnp.int32)
        for s in range(per):
            length = jnp.where(row // heads == s, len_ref[p * per + s], length)
        limit = jnp.where(mine, length * kv - lane, -cols)
        limits.append(limit)
        fails = []
        for b in range(blocks):
            sc = sc_s[p, :, b * lanes : (b + 1) * lanes] * hd ** (-0.5) + offset
            ls = jnp.minimum(sc, 0.0) - jnp.log(1.0 + jnp.exp(-jnp.abs(sc)))
            sg_s[p, :, b * lanes : (b + 1) * lanes] = ls
            fails.append(jnp.where(limit > b * lanes, ls - sc, 0.0))
        failed = jnp.concatenate(fails, axis=0)
        high = failed.astype(BF16)
        low = (failed - high.astype(F32)).astype(BF16)
        hl_s[p] = jnp.concatenate([high, low], axis=1)
    r = lax.broadcasted_iota(jnp.int32, (2 * lanes, 2 * lanes), 0) % lanes
    c = lax.broadcasted_iota(jnp.int32, (2 * lanes, 2 * lanes), 1)
    tri = jnp.where((r > c) | (c >= lanes), 1.0, 0.0).astype(BF16)
    for p in range(pairs):
        sm_s[p] = jnp.dot(hl_s[p], tri, preferred_element_type=F32)
    gains = jnp.concatenate([gain_ref[...]] * per, axis=0)
    for p in range(pairs):
        acc = jnp.zeros((m, lanes), F32)
        weights = [None] * blocks
        for b in reversed(range(blocks)):
            later = sm_s[p, b * m : (b + 1) * m, :lanes] + acc
            acc = acc + sm_s[p, b * m : (b + 1) * m, lanes:]
            weights[b] = jnp.where(
                limits[p] > b * lanes,
                jnp.exp(sg_s[p, :, b * lanes : (b + 1) * lanes] + later),
                0.0,
            )
        weights = jnp.concatenate(weights, axis=1).astype(BF16)
        waits[1][p].wait()
        values = jnp.concatenate([v_s[p * per + s] for s in range(per)], axis=1)
        both = jnp.dot(weights, values, preferred_element_type=F32)
        att = both[:, :hd]
        for s in range(1, per):
            att = jnp.where(row_q // heads == s, both[:, s * hd : (s + 1) * hd], att)
        att = att * lax.rsqrt(jnp.mean(att * att, axis=1, keepdims=True) + EPSILON) * gains
        for s in range(per):
            for h in range(heads):
                ho_s[h, pl.ds(p * per + s, 1), :] = att[s * heads + h : s * heads + h + 1]


def layer_kernel(
    n, nt, kv, per, width, cap,
    x_hbm, g_hbm, wq_hbm, wk_hbm, wv_hbm,
    len_hbm, off_hbm, gain_hbm, fg_hbm, mix_hbm, route_hbm, route_w_hbm,
    key_hbm, val_hbm, wo_hbm, dg_hbm, du_hbm, dd_hbm, eg_hbm, eu_hbm, ed_hbm,
    out_ref, k_ref, v_ref,
    x_ref, g_ref, wq_ref, wk_ref, wv_ref,
    len_ref, off_ref, gain_ref, fg_ref, mix_ref, route_ref, route_w_ref, e_sem,
    k_s, v_s, wo, dg, du, dd, eg, eu, ed, k_sem, v_sem, w_sem,
    p_part, p_got, p_mid, p_got2, p_sums, p_sums_in,
    q_s, sc_s, sg_s, hl_s, sm_s, ho_s,
    heads_all, part, part2, disp, disp_in, sums, sums_in,
    gu, gu_got, gu_mid, gu_got2, hid_all, act_s, share_s,
    ret_x, ret_p, ret, ret_in, res,
    a_in, a_pair, a_cross, a_full, f_in, f_pair, f_cross, f_full,
    *sem_refs,
):
    (p1, p2, ps, hs, ds, ws, ss, g1, g2, i1, i2, rs, as_, fs, xs) = [
        (sem_refs[2 * i], sem_refs[2 * i + 1]) for i in range(len(sem_refs) // 2)
    ]
    g = Grid(n)
    me = g.me
    barrier, greetings = signal_all((("ep", n), ("tp", nt)))
    early = [
        pltpu.make_async_copy(src, dst, e_sem.at[i])
        for i, (src, dst) in enumerate(
            ((x_hbm, x_ref), (g_hbm, g_ref), (wq_hbm, wq_ref), (wk_hbm, wk_ref),
             (wv_hbm, wv_ref), (len_hbm, len_ref), (off_hbm, off_ref), (gain_hbm, gain_ref),
             (fg_hbm, fg_ref), (mix_hbm, mix_ref), (route_hbm, route_ref),
             (route_w_hbm, route_w_ref))
        )
    ]
    for load in early:
        load.start()
    pairs = k_s.shape[0] // per
    k_loads, v_loads = [], []
    for p in range(pairs):
        rng = pl.ds(p * per, per)
        k_loads.append(pltpu.make_async_copy(key_hbm.at[rng], k_s.at[rng], k_sem.at[p]))
        v_loads.append(pltpu.make_async_copy(val_hbm.at[rng], v_s.at[rng], v_sem.at[p]))
    loads = [
        pltpu.make_async_copy(src, dst, w_sem.at[i])
        for i, (src, dst) in enumerate(
            ((wo_hbm, wo), (dg_hbm, dg), (du_hbm, du), (eg_hbm.at[0], eg), (eu_hbm.at[0], eu),
             (ed_hbm.at[0], ed), (dd_hbm, dd))
        )
    ]
    total_rows, block = x_ref.shape
    rows = total_rows // n
    sent = []

    for load in early:
        load.wait()
    for load in k_loads + v_loads + loads:
        load.start()
    x = x_ref[...].astype(F32)
    xg = (x * g_ref[...]).astype(BF16)
    p_sums[...] = row_sums(x * x)
    at = 0
    for w_ref in (wq_ref, wk_ref, wv_ref):
        cols = w_ref.shape[1]
        val = jnp.dot(xg, w_ref[...], preferred_element_type=F32).astype(BF16)
        for i in range(n):
            p_part[i, :, at : at + cols] = val[i * rows : (i + 1) * rows]
        at += cols
    pl.semaphore_wait(barrier, greetings)
    first = scatter_first(g, p_part, p_got, p1)
    p_s = {
        (dz, dx): push("ep", g.at(dz, dx), p_sums.at[pl.ds(0, 1)],
                       p_sums_in.at[dz * g.nx + dx - 1], ps, dz * g.nx + dx - 1)
        for dz, dx in g.peers()
    }
    second = {}
    for dz in spread(g.nz) + [0]:
        second[dz] = scatter_next(g, p_part, p_got, first, p_mid, p_got2, p2, dz)
    total = second.pop(0)
    squares = p_sums[0:1, :]
    for dz, dx in g.peers():
        p_s[dz, dx].wait_recv()
        squares = squares + p_sums_in[dz * g.nx + dx - 1]
    mean = own_column(squares, me * rows, rows) / width
    for dz in second:
        second[dz].wait_recv()
        total = total + p_got2[dz - 1].astype(F32)
    sent += list(first.values()) + list(p_s.values()) + list(second.values())
    total = total * lax.rsqrt(mean + EPSILON)
    hd = q_s.shape[2]
    q_width = wq_ref.shape[1]
    k_width = wk_ref.shape[1]
    for h in range(q_s.shape[0]):
        q_s[h] = total[:, h * hd : (h + 1) * hd].astype(BF16).astype(F32)
    k_ref[...] = total[:, q_width : q_width + k_width].astype(BF16)
    v_ref[...] = total[:, q_width + k_width :].astype(BF16)

    attend(kv, per, (k_loads, v_loads), len_ref, off_ref, gain_ref, q_s, k_s, v_s, sc_s, sg_s,
           hl_s, sm_s, ho_s)
    heads_all[me] = jnp.concatenate(
        [ho_s[h] for h in range(ho_s.shape[0])], axis=1
    ).astype(BF16)
    copies = [
        push("ep", g.at(dz, dx), heads_all.at[me], heads_all.at[me], hs, dz * g.nx + dx - 1)
        for dz, dx in g.peers()
    ]
    sent += copies
    me_t = lax.axis_index("tp")
    core = lax.rem(me_t, 2)
    partner = me_t + 1 - 2 * core
    half = cap // 2
    near = pl.ds(pl.multiple_of(core * half, half), half)
    far = pl.ds(pl.multiple_of((1 - core) * half, half), half)
    top = route_ref.shape[0]
    expert_ids = lax.broadcasted_iota(jnp.int32, (n, total_rows), 0)
    named = [
        jnp.where(route_ref[k : k + 1, :] == expert_ids, 1.0, 0.0).astype(F32)
        for k in range(top)
    ]
    token_r = lax.broadcasted_iota(jnp.int32, (total_rows, total_rows), 0)
    token_c = lax.broadcasted_iota(jnp.int32, (total_rows, total_rows), 1)
    before = jnp.dot(
        sum(named).astype(BF16),
        jnp.where(token_r < token_c, 1.0, 0.0).astype(BF16),
        preferred_element_type=F32,
    )
    slots = [
        jnp.sum(named[k] * before, axis=0, keepdims=True)
        + route_ref[k : k + 1, :].astype(F32) * cap
        for k in range(top)
    ]
    columns = [
        jnp.sum(jnp.where(token_r == token_c, slot, 0.0), axis=1, keepdims=True)
        for slot in slots
    ]
    share_sum = route_w_ref[0:1, :]
    for k in range(1, top):
        share_sum = share_sum + route_w_ref[k : k + 1, :]
    share_rows = [route_w_ref[k : k + 1, :] / share_sum for k in range(top)]
    slot_rows = lax.broadcasted_iota(jnp.int32, (cap, total_rows), 0)
    half_rows = lax.broadcasted_iota(jnp.int32, (half, total_rows), 0) + core * half

    def picks(expert, places):
        place = (places + expert * cap).astype(F32)
        return [slot == place for slot in slots]

    peers = g.peers()
    mine = picks(me, slot_rows)
    hit = functools.reduce(jnp.logical_or, mine)
    chosen = jnp.concatenate(
        [
            jnp.where(functools.reduce(jnp.logical_or, picks(g.at(dz, dx), half_rows)), 1.0, 0.0)
            for dz, dx in peers
        ]
        + [jnp.where(hit, 1.0, 0.0)],
        axis=0,
    ).astype(BF16)
    slot_cols = lax.broadcasted_iota(jnp.int32, (total_rows, half), 1) + core * half

    def returns(expert):
        place = (slot_cols + expert * cap).astype(F32)
        hits = functools.reduce(jnp.logical_or, [column == place for column in columns])
        return jnp.where(hits, 1.0, 0.0).astype(BF16)

    loads[0].wait()
    for copy in copies:
        copy.wait_recv()
    all_heads = heads_all[...].reshape(total_rows, heads_all.shape[2])
    part[...] = jnp.dot(all_heads, wo[...], preferred_element_type=F32).astype(BF16)
    sent += tp_sum(nt, part, a_in, a_pair, a_cross, a_full, as_, None)
    residual = x_ref[...].astype(F32) + a_full[...].astype(F32)
    u = (residual * fg_ref[...]).astype(BF16)
    sums[...] = row_sums(residual * residual)
    res[...] = residual
    packed = jnp.dot(chosen, u, preferred_element_type=F32).astype(BF16)
    d_copies, s_copies = {}, {}
    for j, (dz, dx) in enumerate(peers):
        i = dz * g.nx + dx - 1
        disp[i] = packed[j * half : (j + 1) * half]
        d_copies[i] = push("ep", g.at(dz, dx), disp.at[i], disp_in.at[i, near], ds, i)
    for dz, dx in peers:
        i = dz * g.nx + dx - 1
        s_copies[i] = push("ep", g.at(dz, dx), sums.at[pl.ds(0, 1)], sums_in.at[i], ss, i)
    sent += list(d_copies.values()) + list(s_copies.values())
    own_in = packed[len(peers) * half :]
    hidden = dg.shape[1]
    for load, w, at in ((loads[1], dg, 0), (loads[2], du, hidden)):
        load.wait()
        val = jnp.dot(u, w[...], preferred_element_type=F32).astype(BF16)
        for i in range(n):
            gu[i, :, at : at + hidden] = val[i * rows : (i + 1) * rows]
    g_first = scatter_first(g, gu, gu_got, g1)
    loads[3].wait()
    loads[4].wait()
    span = pl.ds(pl.multiple_of(me * block, block), block)
    gate = jnp.dot(own_in, eg[span, :], preferred_element_type=F32)
    up = jnp.dot(own_in, eu[span, :], preferred_element_type=F32)
    squares = sums[0:1, :]
    order = list(reversed(peers))
    g_order = spread(g.nz) + [0]
    g_second = {}
    forwards = {}
    lead = max(1, len(order) - len(g_order))
    for j in range(len(order) + 1):
        if j < len(order):
            dz, dx = order[j]
            i = dz * g.nx + dx - 1
            d_copies[i].wait_recv()
            forwards[i] = push("tp", partner, disp_in.at[i, near], disp_in.at[i, near], ws, i)
        if 0 <= j - lead < len(g_order):
            dz = g_order[j - lead]
            g_second[dz] = scatter_next(g, gu, gu_got, g_first, gu_mid, gu_got2, g2, dz)
        if j > 0:
            dz, dx = order[j - 1]
            i = dz * g.nx + dx - 1
            s_copies[i].wait_recv()
            squares = squares + sums_in[i]
            forwards[i].wait_recv()
            span = pl.ds(pl.multiple_of(g.source(dz, dx) * block, block), block)
            gate = gate + jnp.dot(disp_in[i], eg[span, :], preferred_element_type=F32)
            up = up + jnp.dot(disp_in[i], eu[span, :], preferred_element_type=F32)
    for dz in g_order:
        if dz not in g_second:
            g_second[dz] = scatter_next(g, gu, gu_got, g_first, gu_mid, gu_got2, g2, dz)
    gate_up = g_second.pop(0)
    sent += list(forwards.values()) + list(g_first.values()) + list(g_second.values())
    scale_row = lax.rsqrt(squares / width + EPSILON)
    scale = jnp.sum(jnp.where(hit, scale_row, 0.0), axis=1, keepdims=True)
    share = jnp.zeros((cap, 1), F32)
    for k in range(len(mine)):
        share = share + jnp.sum(
            jnp.where(mine[k], share_rows[k], 0.0), axis=1, keepdims=True
        )
    gate = gate * scale
    up = up * scale
    act_s[...] = (gate / (1.0 + jnp.exp(-gate)) * up).astype(BF16)
    share_s[...] = jnp.broadcast_to(share, share_s.shape)
    loads[5].wait()
    out = jnp.dot(act_s[far], ed[...], preferred_element_type=F32) * share_s[far][:, 0:1]
    for i in range(n):
        ret_x[i] = out[:, i * block : (i + 1) * block].astype(BF16)
    swap = push("tp", partner, ret_x, ret_p, xs, 0)
    sent.append(swap)
    out = jnp.dot(act_s[near], ed[...], preferred_element_type=F32) * share_s[near][:, 0:1]
    for i in range(n):
        ret[i] = out[:, i * block : (i + 1) * block]
    swap.wait_recv()
    for i in range(n):
        ret_x2 = ret[i] + ret_p[i].astype(F32)
        ret_p[i] = ret_x2.astype(BF16)
    r_copies = {}
    for dz, dx in peers:
        i = dz * g.nx + dx - 1
        r_copies[i] = push("ep", g.at(dz, dx), ret_p.at[g.at(dz, dx)], ret_in.at[i + 1], rs, i)
    sent += list(r_copies.values())
    ret_in[0] = ret_p[me]
    for dz in g_second:
        g_second[dz].wait_recv()
        gate_up = gate_up + gu_got2[dz - 1].astype(F32)
    gate_up = gate_up * own_column(scale_row, me * rows, rows)
    dense_gate = gate_up[:, :hidden]
    hid_all[me] = (dense_gate / (1.0 + jnp.exp(-dense_gate)) * gate_up[:, hidden:]).astype(BF16)
    i_first = {
        dz: push("ep", g.at(dz, 0), hid_all.at[me], hid_all.at[me], i1, dz - 1)
        for dz in spread(g.nz)
    }
    i_second = [
        push("ep", g.at(0, dx), hid_all.at[me], hid_all.at[me], i2, dx - 1)
        for dx in range(1, g.nx)
    ]
    for dz in reversed(spread(g.nz)):
        i_first[dz].wait_recv()
        src = g.source(dz, g.nx)
        for dx in range(1, g.nx):
            i_second.append(
                push("ep", g.at(0, dx), hid_all.at[src], hid_all.at[src], i2,
                     dz * (g.nx - 1) + dx - 1)
            )
    sent += list(i_first.values()) + i_second
    hits = jnp.concatenate(
        [returns(me)]
        + [
            returns(g.source((i + 1) // g.nx, (i + 1) % g.nx))
            for i in range(n - 1)
        ],
        axis=1,
    )
    for i in range(n - 1):
        r_copies[i].wait_recv()
    moe = jnp.dot(hits, ret_in[...].reshape(n * half, block), preferred_element_type=F32)
    loads[6].wait()
    for copy in i_second:
        copy.wait_recv()
    dense = jnp.dot(
        hid_all[...].reshape(total_rows, hidden), dd[...], preferred_element_type=F32
    )
    part2[...] = (moe + mix_ref[...] * dense).astype(BF16)
    sent += tp_sum(nt, part2, f_in, f_pair, f_cross, f_full, fs, res)
    out_ref[...] = f_full[...]
    for copy in sent:
        copy.wait_send()


def finish_kernel(a_ref, b_ref, c_ref, a_out, b_out, c_out, sem):
    copies = [
        pltpu.make_async_copy(src, dst, sem.at[i])
        for i, (src, dst) in enumerate(((a_ref, a_out), (b_ref, b_out), (c_ref, c_out)))
    ]
    for copy in copies:
        copy.start()
    for copy in copies:
        copy.wait()


def per_device(
    n, nt, stream, norm_gain, w_query, w_key, w_value, break_offset, cache_keys, cache_values,
    lengths, w_output, head_gain, ffn_gain, route_experts, route_weights, expert_gate,
    expert_up, expert_down, dense_gate, dense_up, dense_down, mix_gain,
):
    total_rows, block = stream.shape
    width = block * n
    rows = lengths.shape[0]
    kv = cache_keys.shape[2]
    hd = cache_keys.shape[3]
    heads = break_offset.shape[0]
    cache_len = cache_keys.shape[1]
    top = route_experts.shape[1]
    hidden = dense_gate.shape[1]
    expert_hidden = expert_gate.shape[2]
    experts = expert_gate.shape[0] * n
    cap = 2 * rows * top // expert_gate.shape[0]
    assert experts == n
    assert nt % 2 == 0 and cap % 2 == 0
    vmem = pl.BlockSpec(memory_space=pltpu.VMEM)
    hbm = pl.BlockSpec(memory_space=pltpu.HBM)
    dma = pltpu.SemaphoreType.DMA
    vm = pltpu.VMEM
    nz, nx = plan(n)
    per = 2
    flat = kv * cache_len
    pairs = rows // per
    m = per * heads
    blocks = flat // 128
    wide = w_query.shape[1] + w_key.shape[1] + w_value.shape[1]
    dt = w_output.shape[0]
    half_cap = (n, cap // 2, block)
    half_rows = (total_rows // 2, block)
    counts = (
        nz * (nx - 1), nz - 1, n - 1, n - 1, n - 1, n - 1, n - 1, nz * (nx - 1), nz - 1,
        nz - 1, nz * (nx - 1), n - 1, nt // 2 + 1, nt // 2 + 1, 1,
    )
    sems = []
    for count in counts:
        sems += [dma((count,)), dma((count,))]
    operands = (
        stream, norm_gain.reshape(1, block), w_query, w_key, w_value, lengths, break_offset,
        head_gain.reshape(heads, hd), ffn_gain.reshape(1, block), mix_gain.reshape(1, block),
        route_experts.T, route_weights.T,
        cache_keys.reshape(rows, flat, hd), cache_values.reshape(rows, flat, hd),
        w_output, dense_gate, dense_up, dense_down, expert_gate, expert_up, expert_down,
    )
    operands = [pltpu.with_memory_space_constraint(a, pltpu.HBM) for a in operands]
    arrays = pl.pallas_call(
        functools.partial(layer_kernel, n, nt, kv, per, width, cap),
        out_shape=(
            jax.ShapeDtypeStruct((total_rows, block), BF16),
            jax.ShapeDtypeStruct((rows, w_key.shape[1]), BF16),
            jax.ShapeDtypeStruct((rows, w_value.shape[1]), BF16),
        ),
        in_specs=[hbm] * 21,
        out_specs=(vmem, vmem, vmem),
        scratch_shapes=[
            vm(stream.shape, BF16),
            vm((1, block), F32),
            vm(w_query.shape, BF16),
            vm(w_key.shape, BF16),
            vm(w_value.shape, BF16),
            pltpu.SMEM((rows,), jnp.int32),
            pltpu.SMEM((heads,), F32),
            vm((heads, hd), F32),
            vm((1, block), F32),
            vm((1, block), F32),
            vm((top, total_rows), jnp.int32),
            vm((top, total_rows), F32),
            dma((12,)),
            vm((rows, flat, hd), BF16),
            vm((rows, flat, hd), BF16),
            vm(w_output.shape, BF16),
            vm(dense_gate.shape, BF16),
            vm(dense_up.shape, BF16),
            vm(dense_down.shape, BF16),
            vm(expert_gate.shape[1:], BF16),
            vm(expert_up.shape[1:], BF16),
            vm(expert_down.shape[1:], BF16),
            dma((pairs,)),
            dma((pairs,)),
            dma((7,)),
            vm((n, rows, wide), BF16),
            vm((nz * (nx - 1), rows, wide), BF16),
            vm((nz - 1, rows, wide), BF16),
            vm((nz - 1, rows, wide), BF16),
            vm((8, total_rows), F32),
            vm((n - 1, 1, total_rows), F32),
            vm((heads, rows, hd), F32),
            vm((pairs, m, flat), F32),
            vm((pairs, m, flat), F32),
            vm((pairs, blocks * m, 256), BF16),
            vm((pairs, blocks * m, 256), F32),
            vm((heads, rows, hd), F32),
            vm((n, rows, dt), BF16),
            vm((total_rows, block), BF16),
            vm((total_rows, block), BF16),
            vm((n - 1, cap // 2, block), BF16),
            vm((n - 1, cap, block), BF16),
            vm((8, total_rows), F32),
            vm((n - 1, 1, total_rows), F32),
            vm((n, rows, 2 * hidden), BF16),
            vm((nz * (nx - 1), rows, 2 * hidden), BF16),
            vm((nz - 1, rows, 2 * hidden), BF16),
            vm((nz - 1, rows, 2 * hidden), BF16),
            vm((n, rows, hidden), BF16),
            vm((cap, expert_hidden), BF16),
            vm((cap, 128), F32),
            vm(half_cap, BF16),
            vm(half_cap, BF16),
            vm(half_cap, F32),
            vm(half_cap, BF16),
            vm((total_rows, block), F32),
        ]
        + [
            vm(half_rows, BF16),
            vm(half_rows, BF16),
            vm((nt // 2 - 1,) + half_rows, BF16),
            vm((total_rows, block), BF16),
        ] * 2
        + sems,
        compiler_params=pltpu.CompilerParams(
            collective_id=0, has_side_effects=True, vmem_limit_bytes=LIMIT_MIB * 1024 * 1024
        ),
        name="layer",
    )(*operands)
    arrays = [pltpu.with_memory_space_constraint(a, pltpu.VMEM) for a in arrays]
    return pl.pallas_call(
        finish_kernel,
        out_shape=tuple(jax.ShapeDtypeStruct(a.shape, a.dtype) for a in arrays),
        in_specs=[vmem] * 3,
        out_specs=(pl.BlockSpec(memory_space=pl.ANY),) * 3,
        scratch_shapes=[dma((3,))],
        name="finish",
    )(*arrays)


def solution(mesh):
    in_specs = (
        P(None, "ep"),
        P("ep"),
        P("ep", "tp"),
        P("ep", "tp"),
        P("ep", "tp"),
        P("tp"),
        P("ep", None, "tp", None),
        P("ep", None, "tp", None),
        P("ep"),
        P("tp", "ep"),
        P("tp"),
        P("ep"),
        P(),
        P(),
        P("ep", None, "tp"),
        P("ep", None, "tp"),
        P("ep", "tp", None),
        P("ep", "tp"),
        P("ep", "tp"),
        P("tp", "ep"),
        P("ep"),
    )
    out_specs = (P(None, "ep"), P("ep", "tp"), P("ep", "tp"))
    body = functools.partial(per_device, mesh.shape["ep"], mesh.shape["tp"])
    return jax.shard_map(
        body, mesh=mesh, in_specs=in_specs, out_specs=out_specs, check_vma=False
    )
```

time: 81.4 us -> 65.2 us (0.80)
  Pallas kernels: 78.9 us -> 64.4 us
  local copies, waits for them, and re-layouts: 1.57 us -> 0 us
    pallas_call x3 -> x2, Pallas kernels: 78.9 us -> 64.4 us  [the longest x1 63.7 us: per_device(): pl.pallas_call(functools.partial(layer_kernel, n, nt, kv, per, width, cap...]
    unnamed x1 -> x0, local copies, waits for them, and re-layouts: 1.57 us -> none
where the time goes in v1:
time: 65.2 us; the launch traced here: 65 us
  Pallas kernels  64.4 us (99%)
    pallas_call x1, Pallas kernels, per_device(): pl.pallas_call(functools.partial(layer_kernel, n, nt, kv, per, width, cap...  63.7 us

profile of v1, /device:TPU:0, one launch (start us, length us, event | category | flops | bytes accessed | tf_op | source)
XLA Modules:
  0.0 65.0 jit_solution(5827461453238210717)
XLA Ops:
  0.6 63.7 %layer.1 = (bf16[128,512]{1,0:T(8,128)(2,1)S(1)}, bf16[16,256]{1,0:T(8,128)(2,1)S(1)}, bf16[16,256]{1,0:T(8,128)(2,1)S(1)}) custom-call(bf16[128,512]{1,0:T(8,128)(2,1)} %x_hbm.1, f32[1,512]{1,0:T(1,128)} %bitcast.10, bf16[512,512]{1,0:T(8,128)(2,1)} %wq_hbm.1, bf16[512,256]{1,0:T(8,128)(2,1)} %wk_hbm.1, bf16[512,256]{1,0:T(8,128)(2,1)} %wv_hbm.1, ...), custom_call_target="tpu_custom_call" | custom-call | tf_op jit(solution)/shard_map/layer/pallas_call | solution.py:565
  64.3 0.7 %finish.1 = (bf16[128,512]{1,0:T(8,128)(2,1)}, bf16[16,256]{1,0:T(8,128)(2,1)}, bf16[16,256]{1,0:T(8,128)(2,1)}) custom-call(bf16[128,512]{1,0:T(8,128)(2,1)S(1)} %get-tuple-element.6.a_ref, bf16[16,256]{1,0:T(8,128)(2,1)S(1)} %get-tuple-element.7.b_ref, bf16[16,256]{1,0:T(8,128)(2,1)S(1)} %get-tuple-element.8.c_ref), custom_call_target="tpu_custom_call" | custom-call | tf_op jit(solution)/shard_map/finish/pallas_call | solution.py:645

commit v2 on v1

--- a/solution.py
+++ b/solution.py
@@ -77,13 +77,17 @@
     copy = pltpu.make_async_remote_copy(
         src_ref=src,
         dst_ref=dst,
-        send_sem=sems[0].at[i],
-        recv_sem=sems[1].at[i],
+        send_sem=sems[0].at[i if sems[0].shape[0] > 1 else 0],
+        recv_sem=sems[1].at[i if sems[1].shape[0] > 1 else 0],
         device_id={axis: peer},
         device_id_type=MESH,
     )
     copy.start()
     return copy
+
+
+def drain(ref, sems):
+    pltpu.make_async_copy(ref, ref, sems.at[0]).wait()
 
 
 def scatter_first(g, part, got, sems):
@@ -142,6 +146,8 @@
     row_q = lax.broadcasted_iota(jnp.int32, (m, hd), 0)
     row = lax.broadcasted_iota(jnp.int32, (m, lanes), 0)
     lane = lax.broadcasted_iota(jnp.int32, (m, lanes), 1)
+    for load in waits[0]:
+        load.wait()
     for p in range(pairs):
         q = jnp.concatenate(
             [q_s[h, pl.ds(p * per + s, 1), :] for s in range(per) for h in range(heads)], axis=0
@@ -149,7 +155,6 @@
         wide = jnp.concatenate(
             [jnp.where(row_q // heads == s, q, 0.0) for s in range(per)], axis=1
         ).astype(BF16)
-        waits[0][p].wait()
         keys = jnp.concatenate([k_s[p * per + s] for s in range(per)], axis=1)
         sc_s[p] = lax.dot_general(wide, keys, NT, preferred_element_type=F32)
     offset = jnp.zeros((m, lanes), F32)
@@ -179,6 +184,8 @@
     for p in range(pairs):
         sm_s[p] = jnp.dot(hl_s[p], tri, preferred_element_type=F32)
     gains = jnp.concatenate([gain_ref[...]] * per, axis=0)
+    for load in waits[1]:
+        load.wait()
     for p in range(pairs):
         acc = jnp.zeros((m, lanes), F32)
         weights = [None] * blocks
@@ -191,7 +198,6 @@
                 0.0,
             )
         weights = jnp.concatenate(weights, axis=1).astype(BF16)
-        waits[1][p].wait()
         values = jnp.concatenate([v_s[p * per + s] for s in range(per)], axis=1)
         both = jnp.dot(weights, values, preferred_element_type=F32)
         att = both[:, :hd]
@@ -212,15 +218,15 @@
     x_ref, g_ref, wq_ref, wk_ref, wv_ref,
     len_ref, off_ref, gain_ref, fg_ref, mix_ref, route_ref, route_w_ref, e_sem,
     k_s, v_s, wo, dg, du, dd, eg, eu, ed, k_sem, v_sem, w_sem,
-    p_part, p_got, p_mid, p_got2, p_sums, p_sums_in,
+    p_part, p_got, p_mid, p_got2, t_part, t_got, t_mid, t_got2, p_sums, p_sums_in,
     q_s, sc_s, sg_s, hl_s, sm_s, ho_s,
     heads_all, part, part2, disp, disp_in, sums, sums_in,
-    gu, gu_got, gu_mid, gu_got2, hid_all, act_s, share_s,
-    ret_x, ret_p, ret, ret_in, res,
+    gu, gu_got, gu_mid, gu_got2, hid_all,
+    ret_x, ret_p, ret_m, ret_o, ret_y, ret_b, ret, ret_in, res,
     a_in, a_pair, a_cross, a_full, f_in, f_pair, f_cross, f_full,
     *sem_refs,
 ):
-    (p1, p2, ps, hs, ds, ws, ss, g1, g2, i1, i2, rs, as_, fs, xs) = [
+    (p1, p2, t1, t2, ps, hs, ds, ws, ys, ss, g1, g2, i1, i2, rs, as_, fs, xs, bs) = [
         (sem_refs[2 * i], sem_refs[2 * i + 1]) for i in range(len(sem_refs) // 2)
     ]
     g = Grid(n)
@@ -237,10 +243,10 @@
     ]
     for load in early:
         load.start()
-    pairs = k_s.shape[0] // per
+    chunk = k_s.shape[0] // 2
     k_loads, v_loads = [], []
-    for p in range(pairs):
-        rng = pl.ds(p * per, per)
+    for p in range(2):
+        rng = pl.ds(p * chunk, chunk)
         k_loads.append(pltpu.make_async_copy(key_hbm.at[rng], k_s.at[rng], k_sem.at[p]))
         v_loads.append(pltpu.make_async_copy(val_hbm.at[rng], v_s.at[rng], v_sem.at[p]))
     loads = [
@@ -262,57 +268,58 @@
     xg = (x * g_ref[...]).astype(BF16)
     p_sums[...] = row_sums(x * x)
     at = 0
-    for w_ref in (wq_ref, wk_ref, wv_ref):
+    for w_ref, dest in ((wq_ref, p_part), (wk_ref, t_part), (wv_ref, t_part)):
         cols = w_ref.shape[1]
+        at = wk_ref.shape[1] if w_ref is wv_ref else 0
         val = jnp.dot(xg, w_ref[...], preferred_element_type=F32).astype(BF16)
         for i in range(n):
-            p_part[i, :, at : at + cols] = val[i * rows : (i + 1) * rows]
-        at += cols
+            dest[i, :, at : at + cols] = val[i * rows : (i + 1) * rows]
     pl.semaphore_wait(barrier, greetings)
     first = scatter_first(g, p_part, p_got, p1)
-    p_s = {
-        (dz, dx): push("ep", g.at(dz, dx), p_sums.at[pl.ds(0, 1)],
-                       p_sums_in.at[dz * g.nx + dx - 1], ps, dz * g.nx + dx - 1)
-        for dz, dx in g.peers()
-    }
+    for dz, dx in g.peers():
+        i = dz * g.nx + dx - 1
+        push("ep", g.at(dz, dx), p_sums.at[pl.ds(0, 1)], p_sums_in.at[i], ps, i)
+    t_first = scatter_first(g, t_part, t_got, t1)
     second = {}
     for dz in spread(g.nz) + [0]:
         second[dz] = scatter_next(g, p_part, p_got, first, p_mid, p_got2, p2, dz)
     total = second.pop(0)
+    drain(p_sums_in, ps[1])
     squares = p_sums[0:1, :]
-    for dz, dx in g.peers():
-        p_s[dz, dx].wait_recv()
-        squares = squares + p_sums_in[dz * g.nx + dx - 1]
-    mean = own_column(squares, me * rows, rows) / width
+    for i in range(n - 1):
+        squares = squares + p_sums_in[i]
+    inverse = lax.rsqrt(own_column(squares, me * rows, rows) / width + EPSILON)
     for dz in second:
         second[dz].wait_recv()
         total = total + p_got2[dz - 1].astype(F32)
-    sent += list(first.values()) + list(p_s.values()) + list(second.values())
-    total = total * lax.rsqrt(mean + EPSILON)
+    total = total * inverse
     hd = q_s.shape[2]
-    q_width = wq_ref.shape[1]
-    k_width = wk_ref.shape[1]
     for h in range(q_s.shape[0]):
         q_s[h] = total[:, h * hd : (h + 1) * hd].astype(BF16).astype(F32)
-    k_ref[...] = total[:, q_width : q_width + k_width].astype(BF16)
-    v_ref[...] = total[:, q_width + k_width :].astype(BF16)
+    t_second = {}
+    for dz in spread(g.nz) + [0]:
+        t_second[dz] = scatter_next(g, t_part, t_got, t_first, t_mid, t_got2, t2, dz)
+    rows_kv = t_second.pop(0)
 
     attend(kv, per, (k_loads, v_loads), len_ref, off_ref, gain_ref, q_s, k_s, v_s, sc_s, sg_s,
            hl_s, sm_s, ho_s)
     heads_all[me] = jnp.concatenate(
         [ho_s[h] for h in range(ho_s.shape[0])], axis=1
     ).astype(BF16)
-    copies = [
+    for dz, dx in g.peers():
         push("ep", g.at(dz, dx), heads_all.at[me], heads_all.at[me], hs, dz * g.nx + dx - 1)
-        for dz, dx in g.peers()
-    ]
-    sent += copies
+    for dz in t_second:
+        t_second[dz].wait_recv()
+        rows_kv = rows_kv + t_got2[dz - 1].astype(F32)
+    rows_kv = rows_kv * inverse
+    k_ref[...] = rows_kv[:, : k_ref.shape[1]].astype(BF16)
+    v_ref[...] = rows_kv[:, k_ref.shape[1] :].astype(BF16)
     me_t = lax.axis_index("tp")
     core = lax.rem(me_t, 2)
     partner = me_t + 1 - 2 * core
-    half = cap // 2
-    near = pl.ds(pl.multiple_of(core * half, half), half)
-    far = pl.ds(pl.multiple_of((1 - core) * half, half), half)
+    lines = nt // 2
+    part_cap = cap // nt
+    me_y = me_t // 2
     top = route_ref.shape[0]
     expert_ids = lax.broadcasted_iota(jnp.int32, (n, total_rows), 0)
     named = [
@@ -339,8 +346,14 @@
     for k in range(1, top):
         share_sum = share_sum + route_w_ref[k : k + 1, :]
     share_rows = [route_w_ref[k : k + 1, :] / share_sum for k in range(top)]
-    slot_rows = lax.broadcasted_iota(jnp.int32, (cap, total_rows), 0)
-    half_rows = lax.broadcasted_iota(jnp.int32, (half, total_rows), 0) + core * half
+    def slot_of(place):
+        spot = place // part_cap
+        line = lax.rem(me_y + spot % lines, lines)
+        lane_core = jnp.where(spot < lines, 1 - core, core)
+        return (line * 2 + lane_core) * part_cap + place % part_cap
+
+    slot_rows = slot_of(lax.broadcasted_iota(jnp.int32, (cap, total_rows), 0))
+    own_rows = lax.broadcasted_iota(jnp.int32, (part_cap, total_rows), 0) + me_t * part_cap
 
     def picks(expert, places):
         place = (places + expert * cap).astype(F32)
@@ -351,22 +364,24 @@
     hit = functools.reduce(jnp.logical_or, mine)
     chosen = jnp.concatenate(
         [
-            jnp.where(functools.reduce(jnp.logical_or, picks(g.at(dz, dx), half_rows)), 1.0, 0.0)
+            jnp.where(functools.reduce(jnp.logical_or, picks(g.at(dz, dx), own_rows)), 1.0, 0.0)
             for dz, dx in peers
         ]
         + [jnp.where(hit, 1.0, 0.0)],
         axis=0,
     ).astype(BF16)
-    slot_cols = lax.broadcasted_iota(jnp.int32, (total_rows, half), 1) + core * half
-
-    def returns(expert):
-        place = (slot_cols + expert * cap).astype(F32)
-        hits = functools.reduce(jnp.logical_or, [column == place for column in columns])
-        return jnp.where(hits, 1.0, 0.0).astype(BF16)
+    slot_cols = lax.broadcasted_iota(jnp.int32, (total_rows, n * part_cap), 1)
+    source = slot_cols // part_cap
+    source = lax.rem(me // g.nx + g.nz - source // g.nx, g.nz) * g.nx + lax.rem(
+        lax.rem(me, g.nx) + g.nx - source % g.nx, g.nx
+    )
+    slot_cols = (source * cap + me_t * part_cap + slot_cols % part_cap).astype(F32)
+    hits = jnp.where(
+        functools.reduce(jnp.logical_or, [column == slot_cols for column in columns]), 1.0, 0.0
+    ).astype(BF16)
 
     loads[0].wait()
-    for copy in copies:
-        copy.wait_recv()
+    drain(heads_all.at[pl.ds(0, n - 1)], hs[1])
     all_heads = heads_all[...].reshape(total_rows, heads_all.shape[2])
     part[...] = jnp.dot(all_heads, wo[...], preferred_element_type=F32).astype(BF16)
     sent += tp_sum(nt, part, a_in, a_pair, a_cross, a_full, as_, None)
@@ -375,16 +390,15 @@
     sums[...] = row_sums(residual * residual)
     res[...] = residual
     packed = jnp.dot(chosen, u, preferred_element_type=F32).astype(BF16)
-    d_copies, s_copies = {}, {}
+    d_copies = {}
     for j, (dz, dx) in enumerate(peers):
         i = dz * g.nx + dx - 1
-        disp[i] = packed[j * half : (j + 1) * half]
-        d_copies[i] = push("ep", g.at(dz, dx), disp.at[i], disp_in.at[i, near], ds, i)
+        disp[i] = packed[j * part_cap : (j + 1) * part_cap]
+        d_copies[i] = push("ep", g.at(dz, dx), disp.at[i], disp_in.at[i, lines], ds, i)
     for dz, dx in peers:
         i = dz * g.nx + dx - 1
-        s_copies[i] = push("ep", g.at(dz, dx), sums.at[pl.ds(0, 1)], sums_in.at[i], ss, i)
-    sent += list(d_copies.values()) + list(s_copies.values())
-    own_in = packed[len(peers) * half :]
+        push("ep", g.at(dz, dx), sums.at[pl.ds(0, 1)], sums_in.at[i], ss, i)
+    own_in = packed[len(peers) * part_cap :]
     hidden = dg.shape[1]
     for load, w, at in ((loads[1], dg, 0), (loads[2], du, hidden)):
         load.wait()
@@ -401,31 +415,58 @@
     order = list(reversed(peers))
     g_order = spread(g.nz) + [0]
     g_second = {}
-    forwards = {}
-    lead = max(1, len(order) - len(g_order))
-    for j in range(len(order) + 1):
-        if j < len(order):
-            dz, dx = order[j]
-            i = dz * g.nx + dx - 1
-            d_copies[i].wait_recv()
-            forwards[i] = push("tp", partner, disp_in.at[i, near], disp_in.at[i, near], ws, i)
-        if 0 <= j - lead < len(g_order):
-            dz = g_order[j - lead]
-            g_second[dz] = scatter_next(g, gu, gu_got, g_first, gu_mid, gu_got2, g2, dz)
-        if j > 0:
-            dz, dx = order[j - 1]
-            i = dz * g.nx + dx - 1
-            s_copies[i].wait_recv()
-            squares = squares + sums_in[i]
-            forwards[i].wait_recv()
-            span = pl.ds(pl.multiple_of(g.source(dz, dx) * block, block), block)
-            gate = gate + jnp.dot(disp_in[i], eg[span, :], preferred_element_type=F32)
-            up = up + jnp.dot(disp_in[i], eu[span, :], preferred_element_type=F32)
-    for dz in g_order:
-        if dz not in g_second:
-            g_second[dz] = scatter_next(g, gu, gu_got, g_first, gu_mid, gu_got2, g2, dz)
-    gate_up = g_second.pop(0)
-    sent += list(forwards.values()) + list(g_first.values()) + list(g_second.values())
+    y_copies, c_copies = {}, {}
+
+    def arrive(i):
+        d_copies[i].wait_recv()
+        at = disp_in.at[i, lines]
+        c_copies[i, 0] = push("tp", partner, at, disp_in.at[i, 0], ws, i * lines)
+        for k in range(1, lines):
+            y_copies[i, k] = push(
+                "tp", lax.rem(me_t + 2 * k, nt), at, disp_in.at[i, 2 * lines - k], ys,
+                i * (lines - 1) + k - 1,
+            )
+
+    def relay(i):
+        for k in range(1, lines):
+            y_copies[i, k].wait_recv()
+            at = disp_in.at[i, 2 * lines - k]
+            c_copies[i, lines - k] = push(
+                "tp", partner, at, disp_in.at[i, lines - k], ws, i * lines + lines - k
+            )
+
+    def regroup():
+        dz = g_order[len(g_second)]
+        g_second[dz] = scatter_next(g, gu, gu_got, g_first, gu_mid, gu_got2, g2, dz)
+
+    def consume(j):
+        dz, dx = order[j]
+        i = index[j]
+        for k in range(lines):
+            c_copies[i, k].wait_recv()
+        span = pl.ds(pl.multiple_of(g.source(dz, dx) * block, block), block)
+        rows_in = disp_in[i].reshape(cap, block)
+        return (
+            gate + jnp.dot(rows_in, eg[span, :], preferred_element_type=F32),
+            up + jnp.dot(rows_in, eu[span, :], preferred_element_type=F32),
+        )
+
+    index = [dz * g.nx + dx - 1 for dz, dx in order]
+    count = len(index)
+    for i in index:
+        arrive(i)
+    stops = [0, count // 2 + 1]
+    for j, i in enumerate(index):
+        if j in stops:
+            regroup()
+        relay(i)
+    drain(sums_in, ss[1])
+    for i in range(n - 1):
+        squares = squares + sums_in[i]
+    for j in range(count):
+        if j == count // 2 and len(g_second) < len(g_order) - 1:
+            regroup()
+        gate, up = consume(j)
     scale_row = lax.rsqrt(squares / width + EPSILON)
     scale = jnp.sum(jnp.where(hit, scale_row, 0.0), axis=1, keepdims=True)
     share = jnp.zeros((cap, 1), F32)
@@ -435,27 +476,29 @@
         )
     gate = gate * scale
     up = up * scale
-    act_s[...] = (gate / (1.0 + jnp.exp(-gate)) * up).astype(BF16)
-    share_s[...] = jnp.broadcast_to(share, share_s.shape)
+    act = (gate / (1.0 + jnp.exp(-gate)) * up).astype(BF16)
     loads[5].wait()
-    out = jnp.dot(act_s[far], ed[...], preferred_element_type=F32) * share_s[far][:, 0:1]
+    dests = peers + [(0, 0)]
+    swaps, backs, r_copies = [], {}, {}
+    out = jnp.dot(act, ed[...], preferred_element_type=F32) * share
     for i in range(n):
-        ret_x[i] = out[:, i * block : (i + 1) * block].astype(BF16)
-    swap = push("tp", partner, ret_x, ret_p, xs, 0)
-    sent.append(swap)
-    out = jnp.dot(act_s[near], ed[...], preferred_element_type=F32) * share_s[near][:, 0:1]
-    for i in range(n):
-        ret[i] = out[:, i * block : (i + 1) * block]
-    swap.wait_recv()
-    for i in range(n):
-        ret_x2 = ret[i] + ret_p[i].astype(F32)
-        ret_p[i] = ret_x2.astype(BF16)
-    r_copies = {}
-    for dz, dx in peers:
-        i = dz * g.nx + dx - 1
-        r_copies[i] = push("ep", g.at(dz, dx), ret_p.at[g.at(dz, dx)], ret_in.at[i + 1], rs, i)
-    sent += list(r_copies.values())
-    ret_in[0] = ret_p[me]
+        ret_x[i] = out[: cap // 2, i * block : (i + 1) * block].astype(BF16)
+        ret_m[i] = out[cap // 2 :, i * block : (i + 1) * block]
+    for j, (dz, dx) in enumerate(dests):
+        swaps.append(push("tp", partner, ret_x.at[g.at(dz, dx)], ret_p.at[j], xs, j))
+    while len(g_second) < len(g_order):
+        regroup()
+    gate_up = g_second.pop(0)
+    for j, (dz, dx) in enumerate(dests):
+        swaps[j].wait_recv()
+        out = ret_m[g.at(dz, dx)] + ret_p[j].astype(F32)
+        ret_o[j] = out[:part_cap]
+        for k in range(1, lines):
+            ret_y[j, k - 1] = out[k * part_cap : (k + 1) * part_cap].astype(BF16)
+            backs[j, k] = push(
+                "tp", lax.rem(me_t + 2 * k, nt), ret_y.at[j, k - 1], ret_b.at[j, k - 1], bs,
+                j * (lines - 1) + k - 1,
+            )
     for dz in g_second:
         g_second[dz].wait_recv()
         gate_up = gate_up + gu_got2[dz - 1].astype(F32)
@@ -466,41 +509,53 @@
         dz: push("ep", g.at(dz, 0), hid_all.at[me], hid_all.at[me], i1, dz - 1)
         for dz in spread(g.nz)
     }
-    i_second = [
+    for dx in range(1, g.nx):
         push("ep", g.at(0, dx), hid_all.at[me], hid_all.at[me], i2, dx - 1)
-        for dx in range(1, g.nx)
-    ]
-    for dz in reversed(spread(g.nz)):
+    pending = list(reversed(spread(g.nz)))
+
+    def spread_hidden():
+        dz = pending.pop(0)
         i_first[dz].wait_recv()
         src = g.source(dz, g.nx)
         for dx in range(1, g.nx):
-            i_second.append(
-                push("ep", g.at(0, dx), hid_all.at[src], hid_all.at[src], i2,
-                     dz * (g.nx - 1) + dx - 1)
-            )
-    sent += list(i_first.values()) + i_second
-    hits = jnp.concatenate(
-        [returns(me)]
-        + [
-            returns(g.source((i + 1) // g.nx, (i + 1) % g.nx))
-            for i in range(n - 1)
-        ],
-        axis=1,
-    )
-    for i in range(n - 1):
-        r_copies[i].wait_recv()
-    moe = jnp.dot(hits, ret_in[...].reshape(n * half, block), preferred_element_type=F32)
+            push("ep", g.at(0, dx), hid_all.at[src], hid_all.at[src], i2,
+                 dz * (g.nx - 1) + dx - 1)
+
+    for j, (dz, dx) in enumerate(dests):
+        out = ret_o[j]
+        for k in range(1, lines):
+            backs[j, k].wait_recv()
+            out = out + ret_b[j, k - 1].astype(F32)
+        i = dz * g.nx + dx
+        if i == 0:
+            ret_in[0] = out.astype(BF16)
+        else:
+            ret[j] = out.astype(BF16)
+            r_copies[i] = push("ep", g.at(dz, dx), ret.at[j], ret_in.at[i], rs, i - 1)
+        if pending and n - j <= len(pending) + 1:
+            spread_hidden()
+    while pending:
+        spread_hidden()
     loads[6].wait()
-    for copy in i_second:
-        copy.wait_recv()
+    drain(hid_all.at[pl.ds(0, g.nz * (g.nx - 1))], i2[1])
     dense = jnp.dot(
         hid_all[...].reshape(total_rows, hidden), dd[...], preferred_element_type=F32
     )
+    drain(ret_in.at[pl.ds(1, n - 1)], rs[1])
+    moe = jnp.dot(hits, ret_in[...].reshape(n * part_cap, block), preferred_element_type=F32)
     part2[...] = (moe + mix_ref[...] * dense).astype(BF16)
     sent += tp_sum(nt, part2, f_in, f_pair, f_cross, f_full, fs, res)
     out_ref[...] = f_full[...]
     for copy in sent:
         copy.wait_send()
+    for sems, ref in (
+        (p1, p_got), (p2, p_mid), (t1, t_got), (t2, t_mid), (ps, p_sums_in),
+        (hs, heads_all.at[pl.ds(0, n - 1)]), (ds, disp), (ws, disp_in.at[:, pl.ds(0, lines)]),
+        (ys, ret_y.at[pl.ds(0, n - 1)]), (ss, sums_in), (g1, gu_got), (g2, gu_mid),
+        (i1, hid_all.at[pl.ds(0, g.nz - 1)]), (i2, hid_all.at[pl.ds(0, g.nz * (g.nx - 1))]),
+        (rs, ret.at[pl.ds(0, n - 1)]), (xs, ret_x), (bs, ret_y),
+    ):
+        drain(ref, sems[0])
 
 
 def finish_kernel(a_ref, b_ref, c_ref, a_out, b_out, c_out, sem):
@@ -528,11 +583,10 @@
     cache_len = cache_keys.shape[1]
     top = route_experts.shape[1]
     hidden = dense_gate.shape[1]
-    expert_hidden = expert_gate.shape[2]
     experts = expert_gate.shape[0] * n
     cap = 2 * rows * top // expert_gate.shape[0]
     assert experts == n
-    assert nt % 2 == 0 and cap % 2 == 0
+    assert nt % 2 == 0 and cap % nt == 0
     vmem = pl.BlockSpec(memory_space=pltpu.VMEM)
     hbm = pl.BlockSpec(memory_space=pltpu.HBM)
     dma = pltpu.SemaphoreType.DMA
@@ -543,17 +597,17 @@
     pairs = rows // per
     m = per * heads
     blocks = flat // 128
-    wide = w_query.shape[1] + w_key.shape[1] + w_value.shape[1]
     dt = w_output.shape[0]
-    half_cap = (n, cap // 2, block)
+    lines = nt // 2
+    part_cap = cap // nt
     half_rows = (total_rows // 2, block)
+    first, second, relays = nz * (nx - 1), nz - 1, (n - 1) * lines
     counts = (
-        nz * (nx - 1), nz - 1, n - 1, n - 1, n - 1, n - 1, n - 1, nz * (nx - 1), nz - 1,
-        nz - 1, nz * (nx - 1), n - 1, nt // 2 + 1, nt // 2 + 1, 1,
-    )
-    sems = []
-    for count in counts:
-        sems += [dma((count,)), dma((count,))]
+        (1, first), (1, second), (1, first), (1, second), (1, 1), (1, 1), (1, n - 1),
+        (1, relays), (1, relays - n + 1), (1, 1), (1, first), (1, second), (1, second), (1, 1),
+        (1, 1), (lines + 1,) * 2, (lines + 1,) * 2, (1, n), (1, n * (lines - 1)),
+    )
+    sems = [dma((count,)) for pair in counts for count in pair]
     operands = (
         stream, norm_gain.reshape(1, block), w_query, w_key, w_value, lengths, break_offset,
         head_gain.reshape(heads, hd), ffn_gain.reshape(1, block), mix_gain.reshape(1, block),
@@ -594,13 +648,16 @@
             vm(expert_gate.shape[1:], BF16),
             vm(expert_up.shape[1:], BF16),
             vm(expert_down.shape[1:], BF16),
-            dma((pairs,)),
-            dma((pairs,)),
+            dma((2,)),
+            dma((2,)),
             dma((7,)),
-            vm((n, rows, wide), BF16),
-            vm((nz * (nx - 1), rows, wide), BF16),
-            vm((nz - 1, rows, wide), BF16),
-            vm((nz - 1, rows, wide), BF16),
+        ]
+        + [
+            vm((count, rows, cols), BF16)
+            for cols in (w_query.shape[1], w_key.shape[1] + w_value.shape[1])
+            for count in (n, nz * (nx - 1), nz - 1, nz - 1)
+        ]
+        + [
             vm((8, total_rows), F32),
             vm((n - 1, 1, total_rows), F32),
             vm((heads, rows, hd), F32),
@@ -612,8 +669,8 @@
             vm((n, rows, dt), BF16),
             vm((total_rows, block), BF16),
             vm((total_rows, block), BF16),
-            vm((n - 1, cap // 2, block), BF16),
-            vm((n - 1, cap, block), BF16),
+            vm((n - 1, part_cap, block), BF16),
+            vm((n - 1, nt, part_cap, block), BF16),
             vm((8, total_rows), F32),
             vm((n - 1, 1, total_rows), F32),
             vm((n, rows, 2 * hidden), BF16),
@@ -621,12 +678,14 @@
             vm((nz - 1, rows, 2 * hidden), BF16),
             vm((nz - 1, rows, 2 * hidden), BF16),
             vm((n, rows, hidden), BF16),
-            vm((cap, expert_hidden), BF16),
-            vm((cap, 128), F32),
-            vm(half_cap, BF16),
-            vm(half_cap, BF16),
-            vm(half_cap, F32),
-            vm(half_cap, BF16),
+            vm((n, cap // 2, block), BF16),
+            vm((n, cap // 2, block), BF16),
+            vm((n, cap // 2, block), F32),
+            vm((n, part_cap, block), F32),
+            vm((n, lines - 1, part_cap, block), BF16),
+            vm((n, lines - 1, part_cap, block), BF16),
+            vm((n, part_cap, block), BF16),
+            vm((n, part_cap, block), BF16),
             vm((total_rows, block), F32),
         ]
         + [

time: 65.2 us -> 57.2 us (0.88)
  Pallas kernels: 64.4 us -> 56.4 us
    pallas_call x1, Pallas kernels: 63.7 us -> 55.7 us  [per_device(): pl.pallas_call(functools.partial(layer_kernel, n, nt, kv, per, width, cap...]
where the time goes in v2:
time: 57.2 us; the launch traced here: 57 us
  Pallas kernels  56.4 us (99%)
  between operations  0.65 us (1%)
    pallas_call x1, Pallas kernels, per_device(): pl.pallas_call(functools.partial(layer_kernel, n, nt, kv, per, width, cap...  55.7 us

profile of v2, /device:TPU:0, one launch (start us, length us, event | category | flops | bytes accessed | tf_op | source)
XLA Modules:
  0.0 57.0 jit_solution(9107996785738660914)
XLA Ops:
  0.6 55.7 %layer.1 = (bf16[128,512]{1,0:T(8,128)(2,1)S(1)}, bf16[16,256]{1,0:T(8,128)(2,1)S(1)}, bf16[16,256]{1,0:T(8,128)(2,1)S(1)}) custom-call(bf16[128,512]{1,0:T(8,128)(2,1)} %x_hbm.1, f32[1,512]{1,0:T(1,128)} %bitcast.10, bf16[512,512]{1,0:T(8,128)(2,1)} %wq_hbm.1, bf16[512,256]{1,0:T(8,128)(2,1)} %wk_hbm.1, bf16[512,256]{1,0:T(8,128)(2,1)} %wv_hbm.1, ...), custom_call_target="tpu_custom_call" | custom-call | tf_op jit(solution)/shard_map/layer/pallas_call | solution.py:619
  56.3 0.7 %finish.1 = (bf16[128,512]{1,0:T(8,128)(2,1)}, bf16[16,256]{1,0:T(8,128)(2,1)}, bf16[16,256]{1,0:T(8,128)(2,1)}) custom-call(bf16[128,512]{1,0:T(8,128)(2,1)S(1)} %get-tuple-element.6.a_ref, bf16[16,256]{1,0:T(8,128)(2,1)S(1)} %get-tuple-element.7.b_ref, bf16[16,256]{1,0:T(8,128)(2,1)S(1)} %get-tuple-element.8.c_ref), custom_call_target="tpu_custom_call" | custom-call | tf_op jit(solution)/shard_map/finish/pallas_call | solution.py:704
